TPU v7x, 256 devices: a whole 4x4x8 slice. The times are simulated.
256 devices in a mesh: sp: 32 (over z, y), tp: 8 (over x, core).
Axes of the slice: x: 4, y: 4, z: 8, core: 2. Of those that a mesh axis runs over, the one named last changes fastest.
Arguments:
- skip_trunk_vector: bfloat16 [16384, 2048], P('sp', 'tp'), may hold values from -16 to 16
- valve_preactivation: bfloat16 [16384, 2048], P('sp', 'tp'), may hold values from -6 to 6
- projected_heads_payload: bfloat16 [16384, 2048], P('sp', 'tp'), may hold values from -6 to 6
- cluster_ingests: bfloat16 [16384, 1024], P('sp', 'tp'), may hold values from -6 to 6
- cluster_observers: bfloat16 [16384, 1024], P('sp', 'tp'), may hold values from -6 to 6
- pre_softplus_increments: float32 [2, 16384, 32], P(None, 'sp', 'tp'), may hold values from -6 to 6
- attenuation_ln_rate: float32 [2, 32], P(None, 'tp'), may hold values from -13 to -3
- additional_attenuation: float32 [2, 16384, 32], P(None, 'sp', 'tp'), may hold values from -3 to 0
- payload_conv_weights: float32 [7, 2048], P(None, 'tp'), may hold values from -2 to 2
- ingest_conv_weights: float32 [7, 1024], P(None, 'tp'), may hold values from -2 to 2
- observer_conv_weights: float32 [7, 1024], P(None, 'tp'), may hold values from -2 to 2
- valved_cluster_factor: float32 [2048], P('tp'), may hold values from 0.1 to 1.9
- closing_map_matrix: bfloat16 [2048, 2048], P('tp'), may hold values from -0.125 to 0.125
- dense_standardize_factor: float32 [2048], replicated, may hold values from 0.1 to 1.9
- dense_valve_map: bfloat16 [2048, 5120], P('sp', 'tp'), may hold values from -0.125 to 0.125
- dense_payload_map: bfloat16 [2048, 5120], P('sp', 'tp'), may hold values from -0.125 to 0.125
- valve_series_smoother: float32 [3, 5120], P(None, 'tp'), may hold values from -3.5 to 3.5
- payload_series_smoother: float32 [3, 5120], P(None, 'tp'), may hold values from -3.5 to 3.5
- dense_contract_map: bfloat16 [5120, 2048], P('tp', 'sp'), may hold values from -0.078125 to 0.078125
Outputs:
- updated: bfloat16 [16384, 2048], P('sp', 'tp')
All inputs are finite; a program needn't handle non-finite values.
Results may differ from a plain program's by a relative error of at most 0.019.
Values may be sent and summed in bfloat16 or wider, within the bound.
A program may use at most 64 MiB of HBM per device.

v0:
```python
import jax
import jax.numpy as jnp
from jax import lax
from jax.sharding import Mesh
from jax.sharding import PartitionSpec as P

HEADS = 32
GROUPS = 8
STATE = 128
SP = ("sp_0", "sp_1")


EPSILON = 1e-06


def gather_turned(arrays, axis, dims):
    turned = [jnp.moveaxis(a, dim, 0) for a, dim in zip(arrays, dims)]
    both = jnp.concatenate([t.reshape(len(t), -1) for t in turned], axis=1)
    filled, at, outs = (lax.all_gather(both, axis, axis=0, tiled=True), 0, [])
    for t, dim in zip(turned, dims):
        share = filled[:, at : at + t[0].size].reshape(-1, *t.shape[1:])
        outs.append(jnp.moveaxis(share, 0, dim))
        at += t[0].size
    return tuple(outs)


def extended(block, sides, width):
    for axis, dim in sides:
        count = lax.axis_size(axis)
        forward = [(i, i + 1) for i in range(count - 1)]
        backward = [(target, source) for source, target in forward]
        low = lax.ppermute(
            lax.slice_in_dim(block, block.shape[dim] - width, None, axis=dim), axis, forward
        )
        high = lax.ppermute(lax.slice_in_dim(block, 0, width, axis=dim), axis, backward)
        block = jnp.concatenate([low, block, high], axis=dim)
    return block


def neutral_like(array, identity):
    return jax.tree.map(
        lambda part, zero: jnp.zeros_like(part) + jnp.asarray(zero, part.dtype), array, identity
    )


def prefix_by_axis(array, axes, combine, identity, reverse):
    before = start = neutral_like(array, identity)
    running = array
    for axis in reversed(axes):
        length, position = (lax.axis_size(axis), lax.axis_index(axis))
        pieces = jax.tree.map(
            lambda part, kind: lax.all_gather(part.astype(kind), axis),
            running,
            jax.tree.map(lambda a: jnp.bfloat16 if a.dtype == jnp.float32 else a.dtype, array),
        )
        inside, running = (start, start)
        for k in reversed(range(length)) if reverse else range(length):
            passed = k > position if reverse else k < position
            running = combine(
                running, jax.tree.map(lambda part, own: part[k].astype(own.dtype), pieces, array)
            )
            inside = jax.tree.map(lambda new, old: jnp.where(passed, new, old), running, inside)
        before = combine(inside, before)
    return before


def in_blocks(array, dim, length):
    before, after = (array.shape[:dim], array.shape[dim + 1 :])
    return jnp.moveaxis(array.reshape(*before, length, -1, *after), dim, 0)


def sum_at_owner(array, axis, dim):
    pieces = in_blocks(array, dim, lax.axis_size(axis))
    arrived = lax.all_to_all(pieces, axis, split_axis=0, concat_axis=0, tiled=True)
    return arrived.astype(jnp.float32).sum(axis=0)


def in_order(pieces, dim):
    lengths = list(pieces.shape[1:])
    lengths[dim] *= pieces.shape[0]
    return jnp.moveaxis(pieces, 0, dim).reshape(lengths)


def from_everyone(array, axis):
    length = lax.axis_size(axis)
    return lax.all_to_all(
        jnp.broadcast_to(array[None], (length, *array.shape)), axis, 0, 0, tiled=True
    )


def collect(array, axis, dim):
    return in_order(from_everyone(array, axis), dim)


def conv_rows(padded, kernel, length):
    summed = padded[0:length] * kernel[0]
    for offset in range(1, kernel.shape[0]):
        summed = summed + padded[offset : offset + length] * kernel[offset]
    return summed


def split_einsum(pattern, operand, second):
    high_part = operand.astype(jnp.bfloat16)
    low_part = (operand - high_part.astype(jnp.float32)).astype(jnp.bfloat16)
    return jnp.einsum(pattern, high_part, second, preferred_element_type=jnp.float32) + jnp.einsum(
        pattern, low_part, second, preferred_element_type=jnp.float32
    )


def local_way(mixed_vals, inputs_g, readout_g, stride_lengths_change, fading_exponent, per_group):
    sample_total, head_count, head_width = mixed_vals.shape
    group_count = inputs_g.shape[1]
    state_width = inputs_g.shape[2]
    running = jnp.cumsum(fading_exponent, axis=0)
    places = jnp.arange(sample_total, dtype=jnp.int32)
    lower_mask = places[:, None] >= places[None, :]
    log_gaps = running.T[:, :, None] - running.T[:, None, :]
    decays = jnp.exp(jnp.where(lower_mask[None], log_gaps, -jnp.inf))
    group_scores = jnp.einsum(
        "tgn,sgn->gts", readout_g, inputs_g, preferred_element_type=jnp.float32
    )
    scores = jnp.repeat(group_scores, per_group, axis=0)
    weights = scores * decays * stride_lengths_change.T[:, None, :]
    within = split_einsum("hts,shp->thp", weights, mixed_vals)
    to_end = jnp.exp(running[-1][None, :] - running) * stride_lengths_change
    scaled = (to_end[:, :, None] * mixed_vals.astype(jnp.float32)).reshape(
        sample_total, group_count, per_group, head_width
    )
    block_state = split_einsum("sgep,sgn->gepn", scaled, inputs_g).reshape(
        head_count, head_width, state_width
    )
    return (within, running, (jnp.exp(running[-1]), block_state))


def carried_part(readout_g, running, incoming, per_group):
    head_count, head_width, state_width = incoming.shape
    sample_total, group_count = (readout_g.shape[0], readout_g.shape[1])
    grouped_state = incoming.reshape(group_count, per_group, head_width, state_width)
    outer = split_einsum("gepn,tgn->tgep", grouped_state, readout_g).reshape(
        sample_total, head_count, head_width
    )
    return outer * jnp.exp(running)[:, :, None]


def link_states(earlier, later):
    return (earlier[0] * later[0], earlier[1] * later[0][:, None, None] + later[1])


def shards(
    skip_trunk_vector,
    valve_preactivation,
    projected_heads_payload,
    cluster_ingests,
    cluster_observers,
    pre_softplus_increments,
    attenuation_ln_rate,
    additional_attenuation,
    payload_conv_weights,
    ingest_conv_weights,
    observer_conv_weights,
    valved_cluster_factor,
    closing_map_matrix,
    dense_standardize_factor,
    dense_valve_map,
    dense_payload_map,
    valve_series_smoother,
    payload_series_smoother,
    dense_contract_map,
):
    whole_gate, whole_value, whole_down = gather_turned(
        (dense_valve_map, dense_payload_map, dense_contract_map), SP, (0, 0, 1)
    )
    sample_total = skip_trunk_vector.shape[0]
    head_count = pre_softplus_increments.shape[2]
    per_group = HEADS // GROUPS
    joined = jnp.concatenate([projected_heads_payload, cluster_ingests, cluster_observers], axis=1)
    taps_all = jnp.concatenate(
        [payload_conv_weights, ingest_conv_weights, observer_conv_weights], axis=1
    )
    margin = taps_all.shape[0] // 2
    padded = extended(joined, ((SP, 0),), margin)
    convolved = jax.nn.silu(conv_rows(padded.astype(jnp.float32), taps_all, sample_total)).astype(
        jnp.bfloat16
    )
    payload_columns = projected_heads_payload.shape[1]
    input_cols = cluster_ingests.shape[1]
    head_width = payload_columns // head_count
    mixed_vals = convolved[:, :payload_columns].reshape(sample_total, head_count, head_width)
    inputs_g = convolved[:, payload_columns : payload_columns + input_cols].reshape(
        sample_total, input_cols // STATE, STATE
    )
    readout_g = convolved[:, payload_columns + input_cols :].reshape(
        sample_total, input_cols // STATE, STATE
    )
    stride_lengths_change = jax.nn.softplus(pre_softplus_increments)
    fading_exponent = (
        additional_attenuation - stride_lengths_change * jnp.exp(attenuation_ln_rate)[:, None, :]
    )
    within_fwd, running_fwd, summary_fwd = local_way(
        mixed_vals, inputs_g, readout_g, stride_lengths_change[0], fading_exponent[0], per_group
    )
    flipped_readout = readout_g[::-1]
    within_bwd, running_bwd, summary_bwd = local_way(
        mixed_vals[::-1],
        inputs_g[::-1],
        flipped_readout,
        stride_lengths_change[1][::-1],
        fading_exponent[1][::-1],
        per_group,
    )
    identity = (jnp.ones((head_count,), jnp.float32), jnp.zeros_like(summary_fwd[1]))
    incoming_fwd = prefix_by_axis(summary_fwd, SP, link_states, identity, False)
    incoming_bwd = prefix_by_axis(summary_bwd, SP, link_states, identity, True)
    forward = within_fwd + carried_part(readout_g, running_fwd, incoming_fwd[1], per_group)
    backward = (
        within_bwd + carried_part(flipped_readout, running_bwd, incoming_bwd[1], per_group)
    )[::-1]
    gated = (forward + backward).reshape(sample_total, payload_columns) * jax.nn.silu(
        valve_preactivation.astype(jnp.float32)
    )
    grouped = gated.reshape(
        sample_total, payload_columns // (per_group * head_width), per_group * head_width
    )
    standardized = grouped * lax.rsqrt(jnp.mean(grouped * grouped, axis=2, keepdims=True) + EPSILON)
    blending_result = (
        standardized.reshape(sample_total, payload_columns) * valved_cluster_factor
    ).astype(jnp.bfloat16)
    partial_out = jnp.dot(blending_result, closing_map_matrix, preferred_element_type=jnp.float32)
    mapped_vector = sum_at_owner(partial_out.astype(jnp.bfloat16), "tp", 1)
    intermediate_hidden = (skip_trunk_vector.astype(jnp.float32) + mapped_vector).astype(
        jnp.bfloat16
    )
    middle_rows = collect(intermediate_hidden, "tp", 1)
    rows_f = middle_rows.astype(jnp.float32)
    scaled = rows_f * lax.rsqrt(jnp.mean(rows_f * rows_f, axis=1, keepdims=True) + EPSILON)
    normed_rows = (scaled * dense_standardize_factor).astype(jnp.bfloat16)
    gate_sum = jnp.dot(normed_rows, whole_gate, preferred_element_type=jnp.float32)
    value_sum = jnp.dot(normed_rows, whole_value, preferred_element_type=jnp.float32)
    gate_rows = gate_sum.astype(jnp.bfloat16)
    value_rows = value_sum.astype(jnp.bfloat16)
    up_both = jnp.concatenate([gate_rows, value_rows], axis=1)
    up_padded = extended(up_both, ((SP, 0),), 1)
    taps_both = jnp.concatenate([valve_series_smoother, payload_series_smoother], axis=1)
    spread = conv_rows(up_padded.astype(jnp.float32), taps_both, sample_total)
    split_at = gate_rows.shape[1]
    hidden = (jax.nn.silu(spread[:, :split_at]) * spread[:, split_at:]).astype(jnp.bfloat16)
    partial_down = jnp.dot(hidden, whole_down, preferred_element_type=jnp.float32)
    down_sum = sum_at_owner(partial_down.astype(jnp.bfloat16), "tp", 1)
    return (intermediate_hidden.astype(jnp.float32) + down_sum).astype(jnp.bfloat16)


def solution(mesh):
    finer = Mesh(mesh.devices.reshape(8, 4, mesh.shape["tp"]), ("sp_0", "sp_1", "tp"))
    in_specs = (
        P(SP, "tp"),
        P(SP, "tp"),
        P(SP, "tp"),
        P(SP, "tp"),
        P(SP, "tp"),
        P(None, SP, "tp"),
        P(None, "tp"),
        P(None, SP, "tp"),
        P(None, "tp"),
        P(None, "tp"),
        P(None, "tp"),
        P("tp"),
        P("tp", None),
        P(),
        P(SP, "tp"),
        P(SP, "tp"),
        P(None, "tp"),
        P(None, "tp"),
        P("tp", SP),
    )
    out_specs = P(SP, "tp")
    return jax.shard_map(
        shards, mesh=finer, in_specs=in_specs, out_specs=out_specs, check_vma=False
    )
```

profile of v0, /device:TPU:1, one launch (start us, length us, event | category | flops | bytes accessed | tf_op | source)
XLA Modules:
  0.0 295.3 jit_solution(11980838409470273517)
XLA Ops:
  6.5 1.8 pad_maximum_fusion
  8.3 1.0 constant_dynamic-update-slice_fusion.2
  9.3 0.9 constant_dynamic-update-slice_fusion.1
  10.2 0.9 constant_dynamic-update-slice_fusion
  11.2 4.0 %collective-permute-start = (bf16[3,512]{1,0:T(4,128)(2,1)S(1)}, bf16[3,512]{1,0:T(4,128)(2,1)S(1)}, u32[]{:S(2)}, u32[]{:S(2)}) collective-permute-start(bf16[3,512]{1,0:T(4,128)(2,1)S(1)} %get-tuple-element.14), channel_id=1, source_target_pairs={{0,8},{8,16},{16,24},{24,32},{32,40},{40,48},{48,56},{56,64},{64,7... | collective-permute-start | bytes 9224 | tf_op jit(solution)/shard_map/ppermute | solution.py:32
  15.2 1.3 collective-permute-start.1
  16.5 0.7 exp.47
  17.2 0.8 multiply_subtract_fusion
  18.1 1.2 reduce-window.14
  20.1 0.7 constant_dynamic-update-slice_fusion.5
  20.8 8.7 %all-gather.2 = bf16[4,1,4]{2,1,0:T(2,128)(2,1)S(1)} all-gather(bf16[1,1,4]{2,1,0:T(2,128)(2,1)S(1)} %bitcast.351), channel_id=1, replica_groups=mesh['sp_0'=8,'sp_1'=4,'tp'=8] {'sp_1'}, dimensions={0}, use_global_device_ids=true | all-gather | bytes 40 | tf_op jit(solution)/shard_map/all_gather | solution.py:52
  29.5 0.4 rev.15
  29.9 1.2 reduce-window.16
  31.8 5.6 %all-gather.4 = bf16[4,1,4]{2,1,0:T(2,128)(2,1)S(1)} all-gather(bf16[1,1,4]{2,1,0:T(2,128)(2,1)S(1)} %bitcast.352), channel_id=1, replica_groups=mesh['sp_0'=8,'sp_1'=4,'tp'=8] {'sp_1'}, dimensions={0}, use_global_device_ids=true | all-gather | bytes 40 | tf_op jit(solution)/shard_map/all_gather | solution.py:52
  37.4 0.4 rev.16
  37.7 17.7 %all-gather.3 = bf16[8,1,4]{2,1,0:T(2,128)(2,1)S(1)} all-gather(bf16[1,1,4]{2,1,0:T(2,128)(2,1)S(1)} %fusion.125), channel_id=1, replica_groups=mesh['sp_0'=8,'sp_1'=4,'tp'=8] {'sp_0'}, dimensions={0}, use_global_device_ids=true | all-gather | bytes 72 | tf_op jit(solution)/shard_map/all_gather | solution.py:52
  55.5 10.9 %all-gather.5 = bf16[8,1,4]{2,1,0:T(2,128)(2,1)S(1)} all-gather(bf16[1,1,4]{2,1,0:T(2,128)(2,1)S(1)} %fusion.123), channel_id=1, replica_groups=mesh['sp_0'=8,'sp_1'=4,'tp'=8] {'sp_0'}, dimensions={0}, use_global_device_ids=true | all-gather | bytes 72 | tf_op jit(solution)/shard_map/all_gather | solution.py:52
  66.4 0.7 constant_dynamic-update-slice_fusion.4
  67.1 0.7 constant_dynamic-update-slice_fusion.3
  68.4 0.2 copy.32
  68.8 1.1 multiply_convert_fusion
  70.4 0.5 rev.14
  71.3 0.2 fusion.61
  71.5 0.2 fusion.46
  71.7 12.0 %all-gather.1 = bf16[16,64,128]{2,1,0:T(8,128)(2,1)S(1)} all-gather(bf16[4,64,128]{2,1,0:T(8,128)(2,1)S(1)} %fusion.46), channel_id=3, replica_groups=mesh['sp_0'=8,'sp_1'=4,'tp'=8] {'sp_1'}, dimensions={0}, use_global_device_ids=true | all-gather | bytes 327680 | tf_op jit(solution)/shard_map/all_gather | solution.py:52
  83.9 23.8 %all_gather.42 = bf16[8,4,64,128]{3,2,1,0:T(8,128)(2,1)S(1)} all-gather(bf16[1,4,64,128]{3,2,1,0:T(8,128)(2,1)S(1)} %fusion.90), channel_id=1, replica_groups=mesh['sp_0'=8,'sp_1'=4,'tp'=8] {'sp_0'}, dimensions={0}, use_global_device_ids=true | all-gather | bytes 589824 | tf_op jit(solution)/shard_map/all_gather | solution.py:52
  107.6 0.4 fusion.72
  108.0 0.2 fusion.82
  108.2 0.3 fusion.150
  108.5 1.6 fusion.12
  110.1 1.6 fusion.36
  111.7 0.2 fusion.32
  111.9 0.5 rev.17
  112.5 0.2 fusion.85
  112.7 0.2 fusion.45
  112.9 9.7 %all-gather = bf16[16,64,128]{2,1,0:T(8,128)(2,1)S(1)} all-gather(bf16[4,64,128]{2,1,0:T(8,128)(2,1)S(1)} %fusion.45), channel_id=2, replica_groups=mesh['sp_0'=8,'sp_1'=4,'tp'=8] {'sp_1'}, dimensions={0}, use_global_device_ids=true | all-gather | bytes 327680 | tf_op jit(solution)/shard_map/all_gather | solution.py:52
  122.7 19.3 %all_gather.38 = bf16[8,4,64,128]{3,2,1,0:T(8,128)(2,1)S(1)} all-gather(bf16[1,4,64,128]{3,2,1,0:T(8,128)(2,1)S(1)} %fusion.91), channel_id=1, replica_groups=mesh['sp_0'=8,'sp_1'=4,'tp'=8] {'sp_0'}, dimensions={0}, use_global_device_ids=true | all-gather | bytes 589824 | tf_op jit(solution)/shard_map/all_gather | solution.py:52
  142.1 0.4 fusion.78
  142.4 0.2 fusion.88
  142.6 0.3 fusion.141
  143.0 1.6 fusion.11
  144.6 1.6 fusion.42
  146.1 0.3 fusion.30
  146.6 0.5 copy-done.2
  147.1 0.2 multiply_reduce_fusion.1
  147.3 0.8 convolution_convert_fusion
  148.3 54.4 %all_to_all.15 = bf16[8,512,256]{2,1,0:T(8,128)(2,1)S(1)} all-to-all(bf16[8,512,256]{2,1,0:T(8,128)(2,1)S(1)} %bitcast.319), channel_id=1, replica_groups=mesh['sp_0'=8,'sp_1'=4,'tp'=8] {'tp'}, dimensions={0} | all-to-all | bytes 4194304 | tf_op jit(solution)/shard_map/all_to_all | solution.py:74
  202.7 0.3 convert_reduce_fusion.1
  203.3 1.6 broadcast_in_dim.31
  204.8 4.7 %all-to-all-start.1 = ((bf16[8,512,256]{1,2,0:T(8,128)(2,1)}), bf16[8,512,256]{1,2,0:T(8,128)(2,1)S(1)}, u32[]{:S(2)}, u32[]{:S(2)}) async-start(bf16[8,512,256]{1,2,0:T(8,128)(2,1)} %broadcast_in_dim.31), calls=%async_computation.1 | async-start | bytes 4194304 | tf_op jit(solution)/shard_map/all_to_all | solution.py:86
  209.5 26.2 %all-to-all-done.1 = bf16[8,512,256]{1,2,0:T(8,128)(2,1)S(1)} async-done(((bf16[8,512,256]{1,2,0:T(8,128)(2,1)}), bf16[8,512,256]{1,2,0:T(8,128)(2,1)S(1)}, u32[]{:S(2)}, u32[]{:S(2)}) %all-to-all-start.1) | async-done | bytes 2097184 | tf_op jit(solution)/shard_map/all_to_all | solution.py:86
  235.8 0.5 multiply_reduce_fusion
  236.3 1.9 fusion.1
  238.2 4.3 %fusion.24 = bf16[512,640]{1,0:T(8,128)(2,1)S(1)} fusion(bf16[512,2048]{0,1:T(8,128)(2,1)} %fusion.1, bf16[2048,1920]{1,0:T(8,128)(2,1)} %all-gather.8.cloned.1.call-done), kind=kOutput, calls=%fused_computation.33 | convolution fusion | flops 1342504960 | bytes 5373952 | tf_op jit(solution)/shard_map/dot_general | solution.py:238
  242.6 3.6 %fusion.21 = bf16[512,640]{1,0:T(8,128)(2,1)S(1)} fusion(bf16[512,2048]{0,1:T(8,128)(2,1)S(1)} %copy-done.1, bf16[2048,1920]{1,0:T(8,128)(2,1)} %all-gather.8.cloned.1.call-done), kind=kOutput, calls=%fused_computation.32 | convolution fusion | flops 1342504960 | bytes 5373952 | tf_op jit(solution)/shard_map/dot_general | solution.py:237
  246.2 1.3 collective-permute-start.2
  247.5 1.5 collective-permute-start.3
  249.1 2.8 collective-permute-done.3
  251.9 0.3 maximum_convert_fusion
  252.1 0.8 fusion.5
  252.9 3.6 %convolution_convert_fusion.1 = bf16[512,2048]{1,0:T(8,128)(2,1)S(1)} fusion(bf16[2048,1920]{1,0:T(8,128)(2,1)} %all-gather.8.cloned.1.call-done, f32[512,1280]{1,0:T(8,128)S(1)} %fusion.5), kind=kOutput, calls=%fused_computation.13 | convolution fusion | flops 1345191936 | bytes 7340032 | tf_op jit(solution)/shard_map/dot_general | solution.py:247
  256.7 30.7 %all_to_all.16 = bf16[8,512,256]{2,1,0:T(8,128)(2,1)S(1)} all-to-all(bf16[8,512,256]{2,1,0:T(8,128)(2,1)S(1)} %bitcast.320), channel_id=1, replica_groups=mesh['sp_0'=8,'sp_1'=4,'tp'=8] {'tp'}, dimensions={0} | all-to-all | bytes 4194304 | tf_op jit(solution)/shard_map/all_to_all | solution.py:74
  287.4 0.3 convert_reduce_fusion
  287.7 0.8 add_convert_fusion
  (79 shorter events, 4.1 us)
Async XLA Ops:
  6.5 140.8 %copy-start = (bf16[256,2048]{1,0:T(8,128)(2,1)S(1)}, bf16[256,2048]{1,0:T(8,128)(2,1)}, u32[]{:S(2)}) copy-start(bf16[256,2048]{1,0:T(8,128)(2,1)} %param.31) | copy-start | bytes 3145732
  6.5 231.7 %all-gather.8.cloned.1.call-start = ((), (), s32[]{:S(2)}) async-start(), calls=%async_computation.3 | async-start | bytes 8110080 | tf_op jit(solution)/shard_map/all_gather | solution.py:19
  11.2 57.4 %collective-permute-start = (bf16[3,512]{1,0:T(4,128)(2,1)S(1)}, bf16[3,512]{1,0:T(4,128)(2,1)S(1)}, u32[]{:S(2)}, u32[]{:S(2)}) collective-permute-start(bf16[3,512]{1,0:T(4,128)(2,1)S(1)} %get-tuple-element.14), channel_id=1, source_target_pairs={{0,8},{8,16},{16,24},{24,32},{32,40},{40,48},{48,56},{56,64},{64,7... | collective-permute-start | bytes 9224 | tf_op jit(solution)/shard_map/ppermute | solution.py:32
  15.2 53.4 %collective-permute-start.1 = (bf16[3,512]{1,0:T(4,128)(2,1)S(1)}, bf16[3,512]{1,0:T(4,128)(2,1)S(1)}, u32[]{:S(2)}, u32[]{:S(2)}) collective-permute-start(bf16[3,512]{1,0:T(4,128)(2,1)S(1)} %get-tuple-element.15), channel_id=1, source_target_pairs={{8,0},{16,8},{24,16},{32,24},{40,32},{48,40},{56,48},{64,56},{72,6... | collective-permute-start | bytes 9224 | tf_op jit(solution)/shard_map/ppermute | solution.py:35
  68.3 41.8 %copy-start.3 = (pred[512,512]{1,0:T(8,128)(4,1)}, pred[512,512]{1,0:T(8,128)(4,1)S(1)}, u32[]{:S(2)}) copy-start(pred[512,512]{1,0:T(8,128)(4,1)S(1)} %iota_compare_fusion) | copy-start | bytes 786436
  112.4 30.5 %copy-start.4 = (pred[512,512]{1,0:T(8,128)(4,1)S(1)}, pred[512,512]{1,0:T(8,128)(4,1)}, u32[]{:S(2)}) copy-start(pred[512,512]{1,0:T(8,128)(4,1)} %copy-done.3) | copy-start | bytes 786436
  146.1 1.0 copy-start.2
  146.1 1.2 copy-start.9
  148.3 54.8 %copy-start.5 = (bf16[512,256]{1,0:T(8,128)(2,1)S(1)}, bf16[512,256]{1,0:T(8,128)(2,1)}, u32[]{:S(2)}) copy-start(bf16[512,256]{1,0:T(8,128)(2,1)} %param.19) | copy-start | bytes 786436
  204.8 4.7 %copy-start.6 = (f32[3,640]{1,0:T(4,128)S(1)}, f32[3,640]{1,0:T(4,128)}, u32[]{:S(2)}) copy-start(f32[3,640]{1,0:T(4,128)} %param.35) | copy-start | bytes 23044
  204.8 4.7 %copy-start.7 = (f32[3,640]{1,0:T(4,128)S(1)}, f32[3,640]{1,0:T(4,128)}, u32[]{:S(2)}) copy-start(f32[3,640]{1,0:T(4,128)} %param.36) | copy-start | bytes 23044
  204.8 31.4 %copy-start.8 = (f32[2048]{0:T(1024)S(1)}, f32[2048]{0:T(1024)}, u32[]{:S(2)}) copy-start(f32[2048]{0:T(1024)} %param.32) | copy-start | bytes 24580
  204.8 30.9 %all-to-all-start.1 = ((bf16[8,512,256]{1,2,0:T(8,128)(2,1)}), bf16[8,512,256]{1,2,0:T(8,128)(2,1)S(1)}, u32[]{:S(2)}, u32[]{:S(2)}) async-start(bf16[8,512,256]{1,2,0:T(8,128)(2,1)} %broadcast_in_dim.31), calls=%async_computation.1 | async-start | bytes 4194304 | tf_op jit(solution)/shard_map/all_to_all | solution.py:86
  238.2 4.4 %copy-start.1 = (bf16[512,2048]{0,1:T(8,128)(2,1)S(1)}, bf16[512,2048]{0,1:T(8,128)(2,1)}, u32[]{:S(2)}) copy-start(bf16[512,2048]{0,1:T(8,128)(2,1)} %fusion.1) | copy-start | bytes 6291460
  246.2 2.9 collective-permute-start.2
  247.5 4.4 %collective-permute-start.3 = (bf16[1,1280]{1,0:T(2,128)(2,1)S(1)}, bf16[1,1280]{1,0:T(2,128)(2,1)S(1)}, u32[]{:S(2)}, u32[]{:S(2)}) collective-permute-start(bf16[1,1280]{1,0:T(2,128)(2,1)S(1)} %get-tuple-element.9), channel_id=1, source_target_pairs={{8,0},{16,8},{24,16},{32,24},{40,32},{48,40},{56,48},{64,56},{72,6... | collective-permute-start | bytes 7688 | tf_op jit(solution)/shard_map/ppermute | solution.py:35
Sparse Core Ops, SparseCore 0:
  9.9 103.2 all-gather.7
where the time goes:
time: 299 us; the launch traced here: 295 us
  blocking collectives  193 us (65%)
  waiting for transfers between devices  29 us (10%)
  matrix products  21 us (7%)
  between operations  14 us (5%)
  other arithmetic  13.6 us (5%)
  starting transfers between devices  12.8 us (4%)
  local copies, waits for them, and re-layouts  11.9 us (4%)
    all_gather x8, blocking collectives, prefix_by_axis(): lax.all_gather(part.astype(kind), axis)  108 us
    all_to_all x2, blocking collectives, sum_at_owner(): lax.all_to_all(pieces, axis, split_axis=0, concat_axis=0, tiled=True)  85.2 us
    all_to_all x1, waiting for transfers between devices, from_everyone(): lax.all_to_all(jnp.broadcast_to(array[None], (length, *array.shape)), axi...  26.2 us
  transfers between devices with their start and end apart: 6, of which 2 were waited for; matrix products, arithmetic and copies ran while one was open for 10% of the time, Pallas kernels for 0%

commit v1 on v0

v1 whole, which is shorter than its diff:
```python
import jax
import jax.numpy as jnp
from jax import lax
from jax.experimental import pallas as pl
from jax.experimental.pallas import tpu as pltpu
from jax.sharding import Mesh
from jax.sharding import PartitionSpec as P

EPSILON = 1e-06
MESH = pl.DeviceIdType.MESH
NZ, NY, NX = 8, 4, 4
NSP, NTP = NZ * NY, NX * 2
T = 512
CH = 128
HEAD = 64
W_ROWS = 64
ORDER = (0, 3, 1, 2)
F32, BF16 = jnp.float32, jnp.bfloat16


def silu(v):
    return v / (1.0 + jnp.exp(-v))


def layer(
    skip, valve, payload, ingest, observer, pre, rate, extra, taps_p, taps_i, taps_o,
    group_gain, closing, norm_gain, own_w, taps_g, taps_v, out,
    wbuf, wc, xpad, taps, vals, ins, outs, rows, cols, weights, inner,
    dec_src, dec_rcv, st_src, st_rcv, res_src, res_rcv, state_in,
    mix, mid, normed, gate, value, edge_src, edge_rcv, hidden,
    d2d_src, d2d_rcv, own_sum, far_src, far_rcv, near_src, near_rcv,
    s_w, s_small, s_ag,
    r_z, r_y, r_f, r_dy, r_dz, r_small, r_ag, r_d2d, r_far, r_near, s_tail,
):
    z, y = lax.axis_index("z"), lax.axis_index("y")
    x, c = lax.axis_index("x"), lax.axis_index("c")
    sp, tp = z * NY + y, x * 2 + c
    xl, xr, xo = lax.rem(x + 3, NX), lax.rem(x + 1, NX), lax.rem(x + 2, NX)
    zl, zr = lax.rem(z + 7, NZ), lax.rem(z + 1, NZ)
    yl, yr, yo = lax.rem(y + 3, NY), lax.rem(y + 1, NY), lax.rem(y + 2, NY)
    sib = {"c": 1 - c}
    nxt, prv = lax.rem(sp + 1, NSP), lax.rem(sp + NSP - 1, NSP)

    def at_sp(s):
        return {"z": s // NY, "y": lax.rem(s, NY)}

    def rc(src, dst, ssem, rsem, dev):
        return pltpu.make_async_remote_copy(
            src_ref=src, dst_ref=dst, send_sem=ssem, recv_sem=rsem, device_id=dev, device_id_type=MESH
        )

    def got(ref, rsem, dev):
        rc(ref, ref, s_w, rsem, dev).wait_recv()

    def sent(ref, ssem, dev):
        rc(ref, ref, ssem, r_d2d.at[0], dev).wait_send()

    def wrow(zi, yi):
        return pl.ds(pl.multiple_of((zi * NY + yi) * W_ROWS, W_ROWS), W_ROWS)

    def zoff(dz):
        return lax.rem(z + dz, NZ)

    def gv_z_send(k):
        if k == 0:
            a = b = own_w.at[0:2]
            da = db = wbuf.at[0:2, wrow(z, y)]
        else:
            lo, hi = wrow(zoff(8 - k), y), wrow(zoff(k), y)
            if k < 3:
                a = da = wbuf.at[0:2, lo]
                b = db = wbuf.at[0:2, hi]
            else:
                a = da = wbuf.at[0, lo]
                b = db = wbuf.at[1, hi]
        rc(a, da, s_w, r_z.at[0, k], {"z": zr}).start()
        rc(b, db, s_w, r_z.at[1, k], {"z": zl}).start()

    def gv_z_wait(k):
        lo, hi = wrow(zoff(7 - k), y), wrow(zoff(1 + k), y)
        if k < 3:
            got(wbuf.at[0:2, lo], r_z.at[0, k], {"z": zl})
            got(wbuf.at[0:2, hi], r_z.at[1, k], {"z": zr})
        else:
            got(wbuf.at[0, lo], r_z.at[0, k], {"z": zl})
            got(wbuf.at[1, hi], r_z.at[1, k], {"z": zr})

    def gv_y_send(dz):
        dst = wbuf.at[0:2, wrow(zoff(dz), y)]
        src = own_w.at[0:2] if dz == 0 else dst
        rc(src, dst, s_w, r_y.at[0, dz], {"y": yr}).start()
        rc(src, dst, s_w, r_y.at[1, dz], {"y": yl}).start()

    def gv_y_fwd(dz):
        lo, hi = wrow(zoff(dz), yl), wrow(zoff(dz), yr)
        got(wbuf.at[0:2, lo], r_y.at[0, dz], {"y": yl})
        rc(wbuf.at[0, lo], wbuf.at[0, lo], s_w, r_f.at[0, dz], {"y": yr}).start()
        got(wbuf.at[0:2, hi], r_y.at[1, dz], {"y": yr})
        rc(wbuf.at[1, hi], wbuf.at[1, hi], s_w, r_f.at[1, dz], {"y": yl}).start()

    def gv_f_wait(dz):
        far = wrow(zoff(dz), yo)
        got(wbuf.at[0, far], r_f.at[0, dz], {"y": yl})
        got(wbuf.at[1, far], r_f.at[1, dz], {"y": yr})

    def half(zi, yi, h):
        return pl.ds(pl.multiple_of((zi * NY + yi) * W_ROWS + h * 32, 32), 32)

    def dn_y_send():
        dst = wbuf.at[2, wrow(z, y)]
        rc(own_w.at[2], dst, s_w, r_dy.at[0], {"y": yr}).start()
        rc(own_w.at[2], dst, s_w, r_dy.at[1], {"y": yl}).start()

    def dn_y_fwd():
        got(wbuf.at[2, wrow(z, yl)], r_dy.at[0], {"y": yl})
        a = wbuf.at[2, half(z, yl, 0)]
        rc(a, a, s_w, r_dy.at[2], {"y": yr}).start()
        got(wbuf.at[2, wrow(z, yr)], r_dy.at[1], {"y": yr})
        b = wbuf.at[2, half(z, yr, 1)]
        rc(b, b, s_w, r_dy.at[3], {"y": yl}).start()

    def dn_y_wait():
        got(wbuf.at[2, half(z, yo, 0)], r_dy.at[2], {"y": yl})
        got(wbuf.at[2, half(z, yo, 1)], r_dy.at[3], {"y": yr})

    def drow(zi, h=None):
        if h is None:
            return pl.ds(pl.multiple_of(zi * 256, 256), 256)
        return pl.ds(pl.multiple_of(zi * 256 + h * 128, 128), 128)

    def dn_z_send(k):
        ha, hb = (None, None) if k < 3 else (0, 1)
        a = wbuf.at[2, drow(zoff((8 - k) % 8), ha)]
        b = wbuf.at[2, drow(zoff(k), hb)]
        rc(a, a, s_w, r_dz.at[0, k], {"z": zr}).start()
        rc(b, b, s_w, r_dz.at[1, k], {"z": zl}).start()

    def dn_z_wait(k):
        ha, hb = (None, None) if k < 3 else (0, 1)
        got(wbuf.at[2, drow(zoff(7 - k), ha)], r_dz.at[0, k], {"z": zl})
        got(wbuf.at[2, drow(zoff(1 + k), hb)], r_dz.at[1, k], {"z": zr})

    tl, tr, to = xl * 2 + c, xr * 2 + c, xo * 2 + c

    def ag_a(buf, a, r):
        own = buf.at[tp, pl.ds(r * CH, CH)]
        rc(own, own, s_ag.at[a], r_ag.at[a, r, 1], {"x": xr}).start()
        rc(own, own, s_ag.at[a], r_ag.at[a, r, 2], {"x": xl}).start()
        rc(own, own, s_ag.at[a], r_ag.at[a, r, 0], sib).start()

    def ag_b(buf, a, r):
        lo, hi = buf.at[tl, pl.ds(r * CH, CH)], buf.at[tr, pl.ds(r * CH, CH)]
        got(lo, r_ag.at[a, r, 1], {"x": xl})
        fa = buf.at[tl, pl.ds(r * CH, CH // 2)]
        rc(fa, fa, s_ag.at[a], r_ag.at[a, r, 3], {"x": xr}).start()
        rc(lo, lo, s_ag.at[a], r_ag.at[a, r, 5], sib).start()
        got(hi, r_ag.at[a, r, 2], {"x": xr})
        fb = buf.at[tr, pl.ds(r * CH + CH // 2, CH // 2)]
        rc(fb, fb, s_ag.at[a], r_ag.at[a, r, 4], {"x": xl}).start()
        rc(hi, hi, s_ag.at[a], r_ag.at[a, r, 6], sib).start()

    def ag_c(buf, a, r):
        got(buf.at[to, pl.ds(r * CH, CH // 2)], r_ag.at[a, r, 3], {"x": xl})
        got(buf.at[to, pl.ds(r * CH + CH // 2, CH // 2)], r_ag.at[a, r, 4], {"x": xr})
        far = buf.at[to, pl.ds(r * CH, CH)]
        rc(far, far, s_ag.at[a], r_ag.at[a, r, 7], sib).start()

    def ag_d(buf, a, r):
        for kind, xi in ((0, x), (5, xl), (6, xr), (7, xo)):
            got(buf.at[xi * 2 + 1 - c, pl.ds(r * CH, CH)], r_ag.at[a, r, kind], sib)

    barrier = pltpu.get_barrier_semaphore()

    @pl.loop(1, NSP)
    def _(k):
        pl.semaphore_signal(barrier, inc=1, device_id=at_sp(lax.rem(sp + k, NSP)), device_id_type=MESH)

    @pl.loop(1, NTP)
    def _(k):
        d = lax.rem(tp + k, NTP)
        pl.semaphore_signal(
            barrier, inc=1, device_id={"x": d // 2, "c": lax.rem(d, 2)}, device_id_type=MESH
        )

    sign = lax.broadcasted_iota(jnp.int32, (8, 1), 0)
    lane = lax.broadcasted_iota(jnp.int32, (8, T), 1)
    raw = pre[...]
    dt = jnp.maximum(raw, 0.0) + jnp.log1p(jnp.exp(-jnp.abs(raw)))
    decay = extra[...] - dt * jnp.exp(rate[...])
    run = decay
    shift = 1
    while shift < T:
        run = run + jnp.where(lane >= shift, pltpu.roll(run, shift, 1), 0.0)
        shift *= 2
    total = run[:, T - 1 : T]
    forward = sign < 4
    before = jnp.where(lane >= 1, pltpu.roll(run, 1, 1), 0.0)
    place = jnp.where(forward, run, before)
    rows[0:8] = place
    rows[8:16] = dt
    rows[16:24] = jnp.exp(jnp.where(forward, total - run, before)) * dt
    carry_scale = jnp.exp(jnp.where(forward, run, total - before))
    cols[...] = jnp.transpose(jnp.concatenate([place, carry_scale], axis=0), (1, 0))
    block_decay = jnp.exp(total)
    lane1 = lax.broadcasted_iota(jnp.int32, (1, 128), 1)
    for g in range(4):
        first = jnp.broadcast_to(block_decay[2 * g : 2 * g + 1], (1, 128))
        second = jnp.broadcast_to(block_decay[2 * g + 1 : 2 * g + 2], (1, 128))
        dec_src[g] = jnp.where(lane1 < HEAD, first, second)
    dec_rcv[sp] = dec_src[y]
    wbuf[:, wrow(z, y), :] = own_w[...]
    xpad[8 : T + 8, 0:256] = payload[...].astype(F32)
    xpad[8 : T + 8, 256:384] = ingest[...].astype(F32)
    xpad[8 : T + 8, 384:512] = observer[...].astype(F32)
    taps[0:7, 0:256] = taps_p[...]
    taps[0:7, 256:384] = taps_i[...]
    taps[0:7, 384:512] = taps_o[...]
    wc[tp] = closing[:, pl.ds(pl.multiple_of(tp * 256, 256), 256)]

    def conv_strip(r):
        base = pl.multiple_of(r * 16, 16)
        part = xpad[pl.ds(base, 32), :]
        acc = part[5:21] * taps[0:1]
        for i in range(1, 7):
            acc = acc + part[5 + i : 21 + i] * taps[i : i + 1]
        acc = silu(acc).astype(BF16)
        vals[pl.ds(base, 16), :] = acc[:, 0:256]
        ins[pl.ds(base, 16), :] = acc[:, 256:384]
        outs[pl.ds(base, 16), :] = acc[:, 384:512]

    pl.semaphore_wait(barrier, NSP - 1 + NTP - 1)

    rc(xpad.at[T : T + 8], xpad.at[0:8], s_small.at[0], r_small.at[0], at_sp(nxt)).start()
    rc(xpad.at[8:16], xpad.at[T + 8 : T + 16], s_small.at[1], r_small.at[1], at_sp(prv)).start()

    @pl.loop(1, NSP)
    def _(k):
        d = lax.rem(sp + k, NSP)
        rc(dec_src.at[lax.rem(d, NY)], dec_rcv.at[sp], s_small.at[2], r_small.at[2], at_sp(d)).start()

    gv_z_send(0)
    gv_y_send(0)
    dn_y_send()

    @pl.loop(1, NTP)
    def _(k):
        d = lax.rem(tp + k, NTP)
        src = closing.at[:, pl.ds(pl.multiple_of(d * 256, 256), 256)]
        rc(src, wc.at[tp], s_small.at[3], r_small.at[3], {"x": d // 2, "c": lax.rem(d, 2)}).start()

    @pl.loop(1, 31)
    def _(r):
        conv_strip(r)

    got(xpad.at[0:8], r_small.at[0], at_sp(prv))
    got(xpad.at[T + 8 : T + 16], r_small.at[1], at_sp(nxt))
    sent(xpad.at[T : T + 8], s_small.at[0], at_sp(nxt))
    sent(xpad.at[8:16], s_small.at[1], at_sp(prv))
    xpad[0:8] = xpad[0:8] * (sp > 0).astype(F32)
    xpad[T + 8 : T + 16] = xpad[T + 8 : T + 16] * (sp < NSP - 1).astype(F32)
    conv_strip(0)
    conv_strip(31)

    ins_t = jnp.transpose(ins[...].astype(F32), (1, 0))
    lanes = lax.broadcasted_iota(jnp.int32, (128, 128), 1)
    for g in range(4):
        pair = vals[:, (g % 2) * 128 : (g % 2) * 128 + 128]
        first = jnp.dot(
            (ins_t * rows[16 + 2 * g : 17 + 2 * g]).astype(BF16), pair, preferred_element_type=F32
        )
        second = jnp.dot(
            (ins_t * rows[17 + 2 * g : 18 + 2 * g]).astype(BF16), pair, preferred_element_type=F32
        )
        tile = jnp.where(lanes < HEAD, first, second).astype(BF16)
        for i in range(8):
            st_src[4 * i + g] = tile[16 * i : 16 * i + 16]
    st_rcv[sp] = st_src[sp]

    @pl.loop(1, NSP)
    def _(k):
        d = lax.rem(sp + k, NSP)
        rc(st_src.at[d], st_rcv.at[sp], s_small.at[4], r_small.at[4], at_sp(d)).start()

    gv_z_wait(0)
    gv_z_send(1)
    gv_y_send(7)
    gv_y_send(1)

    @pl.loop(0, T // CH)
    def _(tc):
        trows = pl.ds(pl.multiple_of(tc * CH, CH), CH)
        read_t = outs[trows, :]
        at_t = cols[trows, :]
        low = lax.broadcasted_iota(jnp.int32, (CH, CH), 0) - lax.broadcasted_iota(jnp.int32, (CH, CH), 1)
        for sc in range(T // CH):
            scol = slice(sc * CH, sc * CH + CH)
            score = lax.dot_general(
                read_t, ins[scol, :], (((1,), (1,)), ((), ())), preferred_element_type=F32
            )
            gap = low + (tc - sc) * CH
            for h in range(4):
                rf = rows[h : h + 1, scol]
                rb = rows[4 + h : 5 + h, scol]
                df = rows[8 + h : 9 + h, scol]
                db = rows[12 + h : 13 + h, scol]
                gaps = jnp.where(gap >= 0, at_t[:, h : h + 1] - rf, rb - at_t[:, 4 + h : 5 + h])
                step = jnp.where(gap > 0, df, jnp.where(gap < 0, db, df + db))
                weights[h, :, scol] = (score * jnp.exp(gaps) * step).astype(BF16)
        for p in range(2):
            pair = vals[:, p * 128 : p * 128 + 128]
            first = jnp.dot(weights[2 * p], pair, preferred_element_type=F32)
            second = jnp.dot(weights[2 * p + 1], pair, preferred_element_type=F32)
            inner[trows, p * 128 : p * 128 + 128] = jnp.where(lanes < HEAD, first, second)

    gv_y_fwd(0)
    dn_y_fwd()

    got(dec_rcv.at[0 : NSP - 1], r_small.at[2], at_sp(nxt))
    got(st_rcv.at[0 : NSP - 1], r_small.at[4], at_sp(nxt))
    back = y // 2
    carry = jnp.zeros((16, 128), F32)
    for k in range(NSP):
        at = k + back * (NSP - 1 - 2 * k)
        res_src[at] = carry.astype(BF16)
        carry = carry * dec_rcv[at] + st_rcv[at].astype(F32)
    res_rcv[sp] = res_src[sp]

    @pl.loop(1, NSP)
    def _(k):
        d = lax.rem(sp + k, NSP)
        rc(res_src.at[d], res_rcv.at[sp], s_small.at[5], r_small.at[5], at_sp(d)).start()

    gv_z_wait(1)
    gv_z_send(2)
    gv_y_send(6)
    gv_y_send(2)
    gv_y_fwd(7)
    gv_y_fwd(1)
    dn_y_wait()
    got(res_rcv.at[0 : NSP - 1], r_small.at[5], at_sp(nxt))
    for i in range(8):
        for g in range(4):
            state_in[16 * i : 16 * i + 16, 128 * g : 128 * g + 128] = res_rcv[4 * i + g]
    dn_z_send(0)

    for r in ORDER:
        rr = slice(r * CH, r * CH + CH)
        carried = jnp.dot(outs[rr, :], state_in[...], preferred_element_type=F32)
        at_t = cols[rr, :]
        parts = []
        for p in range(2):
            s0 = jnp.where(lanes < HEAD, at_t[:, 8 + 2 * p : 9 + 2 * p], at_t[:, 9 + 2 * p : 10 + 2 * p])
            s1 = jnp.where(lanes < HEAD, at_t[:, 12 + 2 * p : 13 + 2 * p], at_t[:, 13 + 2 * p : 14 + 2 * p])
            pc = slice(128 * p, 128 * p + 128)
            both = inner[rr, pc] + s0 * carried[:, pc] + s1 * carried[:, 256 + 128 * p : 384 + 128 * p]
            parts.append(both * silu(valve[rr, pc].astype(F32)))
        square = jnp.sum(parts[0] * parts[0] + parts[1] * parts[1], axis=1, keepdims=True)
        scale = lax.rsqrt(square * (1.0 / 256) + EPSILON)
        for p in range(2):
            pc = slice(128 * p, 128 * p + 128)
            mix[tp, rr, pc] = (parts[p] * scale * group_gain[0:1, pc]).astype(BF16)
        ag_a(mix, 0, r)

    got(wc.at[0 : NTP - 1], r_small.at[3], sib)

    def project(r):
        rr = slice(r * CH, r * CH + CH)
        acc = skip[rr, :].astype(F32)
        for j in range(NTP):
            acc = acc + jnp.dot(mix[j, rr, :], wc[j], preferred_element_type=F32)
        mid[tp, rr, :] = acc.astype(BF16)
        ag_a(mid, 1, r)

    def norm(n, r):
        @pl.loop(0, CH // 16)
        def _(q):
            rr = pl.ds(pl.multiple_of(r * CH + q * 16, 16), 16)
            square = jnp.zeros((16, 256), F32)
            for j in range(NTP):
                part = mid[j, rr, :].astype(F32)
                square = square + part * part
            scale = lax.rsqrt(jnp.sum(square, axis=1, keepdims=True) * (1.0 / 2048) + EPSILON)
            to_rows = pl.ds(pl.multiple_of(n * CH + q * 16, 16), 16)
            for j in range(NTP):
                jc = slice(256 * j, 256 * j + 256)
                normed[to_rows, jc] = (mid[j, rr, :].astype(F32) * scale * norm_gain[0:1, jc]).astype(BF16)

    r0, r1, r2, r3 = ORDER
    ag_b(mix, 0, r0)
    ag_b(mix, 0, r1)
    ag_c(mix, 0, r0)
    ag_d(mix, 0, r0)
    project(r0)
    gv_z_wait(2)
    gv_z_send(3)
    gv_y_send(5)
    gv_y_send(3)
    ag_b(mix, 0, r2)
    ag_c(mix, 0, r1)
    ag_d(mix, 0, r1)
    project(r1)
    gv_y_fwd(6)
    gv_y_fwd(2)
    ag_b(mix, 0, r3)
    ag_c(mix, 0, r2)
    ag_d(mix, 0, r2)
    project(r2)
    gv_z_wait(3)
    gv_y_send(4)
    dn_z_wait(0)
    dn_z_send(1)
    ag_b(mid, 1, r0)
    ag_c(mix, 0, r3)
    ag_d(mix, 0, r3)
    project(r3)
    gv_y_fwd(5)
    gv_y_fwd(3)
    ag_b(mid, 1, r1)
    ag_c(mid, 1, r0)
    ag_d(mid, 1, r0)
    norm(0, r0)
    ag_b(mid, 1, r2)
    ag_c(mid, 1, r1)
    ag_d(mid, 1, r1)
    norm(1, r1)
    dn_z_wait(1)
    dn_z_send(2)
    gv_y_fwd(4)
    ag_b(mid, 1, r3)
    ag_c(mid, 1, r2)
    ag_d(mid, 1, r2)
    norm(2, r2)
    ag_c(mid, 1, r3)
    ag_d(mid, 1, r3)
    norm(3, r3)
    for dz in range(8):
        gv_f_wait(dz)
    dn_z_wait(2)
    dn_z_send(3)

    def expand(n):
        rr = slice(n * 256, n * 256 + 256)
        for k, dst in ((0, gate), (1, value)):
            res = jnp.dot(normed[rr, :], wbuf[k], preferred_element_type=F32)
            for i in range(2):
                at = ORDER[2 * n + i] * CH + 8
                dst[at : at + CH, :] = res[i * CH : i * CH + CH]

    expand(0)
    edge_src[0, 0:1, :] = gate[T + 7 : T + 8, :]
    edge_src[0, 1:2, :] = value[T + 7 : T + 8, :]
    edge_src[1, 0:1, :] = gate[8:9, :]
    edge_src[1, 1:2, :] = value[8:9, :]
    rc(edge_src.at[0], edge_rcv.at[0], s_tail.at[0], r_small.at[6], at_sp(nxt)).start()
    rc(edge_src.at[1], edge_rcv.at[1], s_tail.at[1], r_small.at[7], at_sp(prv)).start()
    expand(1)

    def hidden_strip(r):
        base = pl.multiple_of(r * 16, 16)
        g, v = gate[pl.ds(base, 32), :], value[pl.ds(base, 32), :]
        gc = g[7:23] * taps_g[0:1] + g[8:24] * taps_g[1:2] + g[9:25] * taps_g[2:3]
        vc = v[7:23] * taps_v[0:1] + v[8:24] * taps_v[1:2] + v[9:25] * taps_v[2:3]
        hidden[pl.ds(base, 16), :] = (silu(gc) * vc).astype(BF16)

    @pl.loop(1, 31)
    def _(r):
        hidden_strip(r)

    got(edge_rcv.at[0], r_small.at[6], at_sp(prv))
    got(edge_rcv.at[1], r_small.at[7], at_sp(nxt))
    has_prv, has_nxt = (sp > 0).astype(F32), (sp < NSP - 1).astype(F32)
    gate[7:8, :] = edge_rcv[0, 0:1, :] * has_prv
    value[7:8, :] = edge_rcv[0, 1:2, :] * has_prv
    gate[T + 8 : T + 9, :] = edge_rcv[1, 0:1, :] * has_nxt
    value[T + 8 : T + 9, :] = edge_rcv[1, 1:2, :] * has_nxt
    hidden_strip(0)
    hidden_strip(31)
    dn_z_wait(3)

    def part_of(xi, ci):
        at = pl.multiple_of((xi * 2 + ci) * 256, 256)
        return lax.dot_general(
            hidden[...], wbuf[2, pl.ds(at, 256), :], (((1,), (1,)), ((), ())), preferred_element_type=F32
        )

    targets = (xo, xr, xl, x)
    for i in range(4):
        d2d_src[i] = part_of(targets[i], 1 - c).astype(BF16)
        rc(d2d_src.at[i], d2d_rcv.at[i], s_tail.at[2], r_d2d.at[i], sib).start()

    def chip_sum(i):
        own = part_of(targets[i], c)
        got(d2d_rcv.at[i], r_d2d.at[i], sib)
        return own + d2d_rcv[i].astype(F32)

    H = T // 2
    far_src[...] = chip_sum(0).astype(BF16)
    rc(far_src.at[0:H], far_rcv.at[0:H], s_tail.at[3], r_far.at[0], {"x": xr}).start()
    rc(far_src.at[H:T], far_rcv.at[H:T], s_tail.at[3], r_far.at[1], {"x": xl}).start()
    right = chip_sum(1)
    near_src[0, H:T] = right[H:T].astype(BF16)
    rc(near_src.at[0, H:T], near_rcv.at[0, H:T], s_tail.at[4], r_near.at[0], {"x": xr}).start()
    own_sum[0:H] = right[0:H]
    left = chip_sum(2)
    near_src[1, 0:H] = left[0:H].astype(BF16)
    rc(near_src.at[1, 0:H], near_rcv.at[1, 0:H], s_tail.at[4], r_near.at[1], {"x": xl}).start()
    own_sum[H:T] = left[H:T]
    got(far_rcv.at[0:H], r_far.at[0], {"x": xl})
    near_src[0, 0:H] = (own_sum[0:H] + far_rcv[0:H].astype(F32)).astype(BF16)
    rc(near_src.at[0, 0:H], near_rcv.at[0, 0:H], s_tail.at[4], r_near.at[2], {"x": xr}).start()
    got(far_rcv.at[H:T], r_far.at[1], {"x": xr})
    near_src[1, H:T] = (own_sum[H:T] + far_rcv[H:T].astype(F32)).astype(BF16)
    rc(near_src.at[1, H:T], near_rcv.at[1, H:T], s_tail.at[4], r_near.at[3], {"x": xl}).start()
    own_sum[...] = chip_sum(3) + mid[tp].astype(F32)
    got(near_rcv.at[0, H:T], r_near.at[0], {"x": xl})
    got(near_rcv.at[1, 0:H], r_near.at[1], {"x": xr})
    got(near_rcv.at[0, 0:H], r_near.at[2], {"x": xl})
    got(near_rcv.at[1, H:T], r_near.at[3], {"x": xr})
    out[...] = (own_sum[...] + near_rcv[0].astype(F32) + near_rcv[1].astype(F32)).astype(BF16)

    sent(dec_rcv.at[0 : NSP - 1], s_small.at[2], at_sp(nxt))
    sent(wc.at[0 : NTP - 1], s_small.at[3], sib)
    sent(st_rcv.at[0 : NSP - 1], s_small.at[4], at_sp(nxt))
    sent(res_rcv.at[0 : NSP - 1], s_small.at[5], at_sp(nxt))
    sent(wbuf.at[:, 0 : 31 * W_ROWS], s_w, {"z": zr})
    sent(mix.at[0:7], s_ag.at[0], sib)
    sent(mid.at[0:7], s_ag.at[1], sib)
    sent(edge_src.at[0], s_tail.at[0], at_sp(nxt))
    sent(edge_src.at[1], s_tail.at[1], at_sp(prv))
    sent(d2d_src, s_tail.at[2], sib)
    sent(far_src, s_tail.at[3], {"x": xr})
    sent(near_src, s_tail.at[4], {"x": xr})


def shards(
    skip, valve, payload, ingest, observer, pre, rate, extra, taps_p, taps_i, taps_o,
    group_gain, closing, norm_gain, w_gate, w_value, taps_g, taps_v, w_down,
):
    own_w = jnp.stack([w_gate, w_value, w_down.T])
    pre_r = jnp.transpose(pre, (0, 2, 1)).reshape(8, T)
    extra_r = jnp.transpose(extra, (0, 2, 1)).reshape(8, T)
    V, D = pltpu.VMEM, pltpu.SemaphoreType.DMA
    scratch = [
        V((3, 2048, 640), BF16),
        V((NTP, 256, 256), BF16),
        V((T + 16, 512), F32),
        V((8, 512), F32),
        V((T, 256), BF16),
        V((T, 128), BF16),
        V((T, 128), BF16),
        V((24, T), F32),
        V((T, 16), F32),
        V((4, CH, T), BF16),
        V((T, 256), F32),
        V((4, 1, 128), F32),
        V((NSP, 1, 128), F32),
        V((NSP, 16, 128), BF16),
        V((NSP, 16, 128), BF16),
        V((NSP, 16, 128), BF16),
        V((NSP, 16, 128), BF16),
        V((128, 512), BF16),
        V((NTP, T, 256), BF16),
        V((NTP, T, 256), BF16),
        V((T, 2048), BF16),
        V((T + 16, 640), F32),
        V((T + 16, 640), F32),
        V((2, 8, 640), F32),
        V((2, 8, 640), F32),
        V((T, 640), BF16),
        V((4, T, 256), BF16),
        V((4, T, 256), BF16),
        V((T, 256), F32),
        V((T, 256), BF16),
        V((T, 256), BF16),
        V((2, T, 256), BF16),
        V((2, T, 256), BF16),
        D,
        D((6,)),
        D((2,)),
        D((2, 4)),
        D((2, 8)),
        D((2, 8)),
        D((4,)),
        D((2, 4)),
        D((8,)),
        D((2, 4, 8)),
        D((4,)),
        D((2,)),
        D((4,)),
        D((5,)),
    ]
    return pl.pallas_call(
        layer,
        out_shape=jax.ShapeDtypeStruct((T, 256), BF16),
        in_specs=[pl.BlockSpec(memory_space=pltpu.VMEM)] * 17,
        out_specs=pl.BlockSpec(memory_space=pltpu.VMEM),
        scratch_shapes=scratch,
        compiler_params=pltpu.CompilerParams(
            collective_id=0, has_side_effects=True, vmem_limit_bytes=60 * 1024 * 1024
        ),
    )(
        skip, valve, payload, ingest, observer, pre_r, rate.reshape(8, 1), extra_r, taps_p, taps_i, taps_o,
        group_gain.reshape(1, 256), closing, norm_gain.reshape(1, 2048), own_w, taps_g, taps_v,
    )


def solution(mesh):
    finer = Mesh(mesh.devices.reshape(NZ, NY, NX, 2), ("z", "y", "x", "c"))
    SP, TP = ("z", "y"), ("x", "c")
    in_specs = (
        P(SP, TP),
        P(SP, TP),
        P(SP, TP),
        P(SP, TP),
        P(SP, TP),
        P(None, SP, TP),
        P(None, TP),
        P(None, SP, TP),
        P(None, TP),
        P(None, TP),
        P(None, TP),
        P(TP),
        P(TP, None),
        P(),
        P(SP, TP),
        P(SP, TP),
        P(None, TP),
        P(None, TP),
        P(TP, SP),
    )
    return jax.shard_map(
        shards, mesh=finer, in_specs=in_specs, out_specs=P(SP, TP), check_vma=False
    )
```

time: 299 us -> 98.2 us (0.33); the launches traced: 295 us -> 97.9 us
  blocking collectives: 193 us -> 0 us
  Pallas kernels: 0 us -> 90.5 us
  waiting for transfers between devices: 29 us -> 0 us
  matrix products: 21 us -> 0 us
  between operations: 14 us -> 0.01 us
  starting transfers between devices: 12.8 us -> 0 us
  other arithmetic: 13.6 us -> 1.65 us
  local copies, waits for them, and re-layouts: 11.9 us -> 5.7 us
    all_gather x8 -> x0, blocking collectives: 108 us -> none  [prefix_by_axis(): lax.all_gather(part.astype(kind), axis)]
    pallas_call x0 -> x1, Pallas kernels: none -> 90.5 us  [shards(): pl.pallas_call(layer, out_shape=jax.ShapeDtypeStruct((T, 256), BF16), in_...]
    all_to_all x2 -> x0, blocking collectives: 85.2 us -> none  [sum_at_owner(): lax.all_to_all(pieces, axis, split_axis=0, concat_axis=0, tiled=True)]
    all_to_all x1 -> x0, waiting for transfers between devices: 26.2 us -> none  [from_everyone(): lax.all_to_all(jnp.broadcast_to(array[None], (length, *array.shape)), axi...]
    dot_general x18 -> x0, matrix products: 21 us -> none  [the longest x1 4.35 us: shards(): jnp.dot(normed_rows, whole_value, preferred_element_type=jnp.float32)]
    ppermute x4 -> x0, starting transfers between devices: 8.11 us -> none  [the longest x2 5.31 us: extended(): lax.ppermute(lax.slice_in_dim(block, block.shape[dim] - width, None, axis...]
    convert_element_type x15 -> x0, other arithmetic: 4.96 us -> none  [the longest x1 1.94 us: shards(): normed_rows = (scaled * dense_standardize_factor).astype(jnp.bfloat16)]
    all_to_all x1 -> x0, starting transfers between devices: 4.68 us -> none  [from_everyone(): lax.all_to_all(jnp.broadcast_to(array[None], (length, *array.shape)), axi...]
  transfers between devices with their start and end apart: 6 -> 0, of which waited for: 2 -> 0; matrix products, arithmetic and copies ran while one was open for 10% -> 0% of each run, Pallas kernels for 0% -> 0%
where the time goes in v1:
time: 98.2 us; the launch traced here: 97.9 us
  Pallas kernels  90.5 us (92%)
  local copies, waits for them, and re-layouts  5.7 us (6%)
  other arithmetic  1.65 us (2%)
    pallas_call x1, Pallas kernels, shards(): pl.pallas_call(layer, out_shape=jax.ShapeDtypeStruct((T, 256), BF16), in_...  90.5 us

profile of v1, /device:TPU:1, one launch (start us, length us, event | category | flops | bytes accessed | tf_op | source)
XLA Modules:
  0.0 97.9 jit_solution(7753895597140905544)
XLA Ops:
  0.0 0.0 copy-start
  0.0 1.4 %reshape.20.rate = f32[8,1]{1,0:T(8,128)} reshape(f32[2,4]{1,0:T(2,128)} %param.25) | data formatting | bytes 64 | tf_op jit(solution)/shard_map/reshape | solution.py:602
  1.4 1.3 %reshape.15.pre = f32[8,512]{1,0:T(8,128)} reshape(f32[2,4,512]{2,1,0:T(4,128)} %bitcast.12) | data formatting | bytes 32768 | tf_op jit(solution)/shard_map/reshape | solution.py:540
  2.7 1.3 %reshape.17.extra = f32[8,512]{1,0:T(8,128)} reshape(f32[2,4,512]{2,1,0:T(4,128)} %bitcast.13) | data formatting | bytes 32768 | tf_op jit(solution)/shard_map/reshape | solution.py:541
  4.0 0.0 copy-done
  4.0 1.7 %pad_maximum_fusion.own_w = bf16[3,64,640]{2,1,0:T(8,128)(2,1)} fusion(bf16[1,64,640]{2,1,0:T(8,128)(2,1)S(1)} %bitcast.9, bf16[1,64,640]{2,1,0:T(8,128)(2,1)} %bitcast.10, bf16[1,64,640]{2,1,0:T(8,128)(2,1)} %bitcast.11), kind=kLoop, calls=%fused_computation | loop fusion | flops 245760 | bytes 491520 | tf_op jit(solution)/shard_map/stack | solution.py:539
  5.7 90.5 %shard_map.181 = bf16[512,256]{1,0:T(8,128)(2,1)} custom-call(bf16[512,256]{1,0:T(8,128)(2,1)} %skip.1, bf16[512,256]{1,0:T(8,128)(2,1)} %valve.1, bf16[512,256]{1,0:T(8,128)(2,1)} %payload.1, bf16[512,128]{1,0:T(8,128)(2,1)} %ingest.1, bf16[512,128]{1,0:T(8,128)(2,1)} %observer.1, f32[8,512]{1,0:T(8,128)} %reshape.15.pre, f32[8,1]{1,0:T(8,128)} %reshape.20.rate, ...), custom_call_target="tpu_custom_call" | custom-call | tf_op jit(solution)/shard_map/pallas_call | solution.py:592
  96.2 1.7 %copy.22 = bf16[512,256]{1,0:T(8,128)(2,1)} copy(bf16[512,256]{1,0:T(8,128)(2,1)} %shard_map.181) | data formatting | bytes 524288
Async XLA Ops:
  0.0 4.0 %copy-start = (bf16[640,64]{0,1:T(8,128)(2,1)S(1)}, bf16[640,64]{0,1:T(8,128)(2,1)}, u32[]{:S(2)}) copy-start(bf16[640,64]{0,1:T(8,128)(2,1)} %param.37) | copy-start | bytes 245764
